TPU v7x, 256 devices: a whole 4x4x8 slice. The times are simulated.
256 devices in a mesh: sp: 32 (over z, y), tp: 8 (over x, core).
Axes of the slice: x: 4, y: 4, z: 8, core: 2. Of those that a mesh axis runs over, the one named last changes fastest.
Arguments:
- residual_in: bfloat16 [12288, 2048], P(('sp', 'tp')), may hold values from -6 to 6
- queries: bfloat16 [12288, 2048], P('sp', 'tp'), may hold values from -180 to 180
- keys: bfloat16 [12288, 2048], P('sp', 'tp'), may hold values from -9 to 9
- values: bfloat16 [12288, 2048], P('sp', 'tp'), may hold values from -6 to 6
- mix_lambda: float32 [16], P('tp'), may hold values from 0.3 to 0.8
- head_gain: float32 [128], replicated, may hold values from 0.1 to 1.9
- out_weight: bfloat16 [2048, 2048], P('tp'), may hold values from -0.125 to 0.125
- norm_gain: float32 [2048], replicated, may hold values from 0.1 to 1.9
- gate_weight: bfloat16 [2048, 5632], P('sp', 'tp'), may hold values from -0.125 to 0.125
- up_weight: bfloat16 [2048, 5632], P('sp', 'tp'), may hold values from -0.125 to 0.125
- down_weight: bfloat16 [5632, 2048], P('tp', 'sp'), may hold values from -0.078125 to 0.078125
Outputs:
- layer_out: bfloat16 [12288, 2048], P(('sp', 'tp'))
All inputs are finite; a program needn't handle non-finite values.
Results may differ from a plain program's by a relative error of at most 0.014.
Values may be sent and summed in bfloat16 or wider, within the bound.
No kernel may reach another device: no remote copies, remote signals or barrier semaphores. Data moves between devices by JAX's collectives and lax.ppermute only.
A program may use at most 128 MiB of HBM per device.

v0:
```python
import math
import jax
import jax.numpy as jnp
from jax import lax
from jax.sharding import PartitionSpec as P

DH = 64
VD = 128


def cut_along(value, dim, devices):
    shape = value.shape
    parts = value.reshape(*shape[:dim], devices, shape[dim] // devices, *shape[dim + 1 :])
    return jnp.moveaxis(parts, dim, 0)


def sent_and_summed(value, axis, dim):
    parts = cut_along(value, dim, lax.axis_size(axis))
    arrived = lax.all_to_all(parts, axis, split_axis=0, concat_axis=0, tiled=True)
    return arrived.astype(jnp.float32).sum(axis=0)


def sent_to_all(value, axis):
    copies = jnp.broadcast_to(value, (lax.axis_size(axis), *value.shape))
    return lax.all_to_all(copies, axis, split_axis=0, concat_axis=0, tiled=True)


def joined_along(parts, dim):
    shape = list(parts.shape[1:])
    shape[dim] *= parts.shape[0]
    return jnp.moveaxis(parts, 0, dim).reshape(shape)


def collect(value, axis, dim):
    parts = sent_to_all(value, axis)
    return joined_along(parts, dim)


def rows_first(arrays, axis, dims):
    turned = [jnp.moveaxis(a, dim, 0) for a, dim in zip(arrays, dims)]
    widths = [t[0].size for t in turned]
    both = jnp.concatenate([t.reshape(-1, w) for t, w in zip(turned, widths)], axis=1)
    result = lax.all_gather(both, axis, axis=0, tiled=True)
    parts = jnp.split(result, [sum(widths[:k]) for k in range(1, len(widths))], axis=1)
    return tuple(
        (
            jnp.moveaxis(b.reshape(-1, *t.shape[1:]), 0, dim)
            for b, t, dim in zip(parts, turned, dims)
        )
    )


def body(
    residual_in,
    queries,
    keys,
    values,
    mix_lambda,
    head_gain,
    out_weight,
    norm_gain,
    gate_weight,
    up_weight,
    down_weight,
):
    tok_local = queries.shape[0]
    heads_local = mix_lambda.shape[0]
    query_four = queries.reshape(tok_local, heads_local, 2, DH)
    inverse_root = 1.0 / math.sqrt(DH)

    def one_block(state, block):
        top, total, weighted = state
        key_block, value_block = block
        scores = (
            jnp.einsum("qhcd,khcd->hcqk", query_four, key_block, preferred_element_type=jnp.float32)
            * inverse_root
        )
        new_top = jnp.maximum(top, jnp.max(scores, axis=-1))
        rescale = jnp.exp(top - new_top)
        expo = jnp.exp(scores - new_top[..., None])
        total = total * rescale + jnp.sum(expo, axis=-1)
        weighted = weighted * rescale[..., None] + jnp.einsum(
            "hcqk,khe->hcqe",
            expo.astype(jnp.bfloat16),
            value_block,
            preferred_element_type=jnp.float32,
        )
        return ((new_top, total, weighted), None)

    start_state = (
        jnp.full((heads_local, 2, tok_local), -1e30, jnp.float32),
        jnp.zeros((heads_local, 2, tok_local), jnp.float32),
        jnp.zeros((heads_local, 2, tok_local, VD), jnp.float32),
    )
    key_piece = lax.all_gather(keys, "sp", axis=0, tiled=True)
    value_piece = lax.all_gather(values, "sp", axis=0, tiled=True)
    count = key_piece.shape[0]
    shards = max(count // tok_local, 1)
    unit = count // shards
    group = max(
        (g for g in range(1, shards + 1) if shards % g == 0 and g * unit <= max(1536, unit))
    )
    width = group * unit
    blocks = count // width
    key_blocks = key_piece.reshape(blocks, width, heads_local, 2, DH)
    value_blocks = value_piece.reshape(blocks, width, heads_local, VD)
    state, unused = lax.scan(one_block, start_state, (key_blocks, value_blocks))
    top, total, weighted = state
    maps = weighted / total[..., None]
    mixed = maps[:, 0] - mix_lambda[:, None, None] * maps[:, 1]
    head_scale = lax.rsqrt(jnp.mean(mixed * mixed, axis=-1, keepdims=True) + 1e-06)
    head_out = (mixed * head_scale * head_gain).astype(jnp.bfloat16)
    attended = jnp.transpose(head_out, (1, 0, 2)).reshape(tok_local, heads_local * VD)
    picked = attended
    projected = sent_and_summed(
        jnp.dot(picked, out_weight, preferred_element_type=jnp.float32).astype(jnp.bfloat16),
        "tp",
        0,
    )
    after_mix = residual_in.astype(jnp.float32) + projected
    row_scale = lax.rsqrt(jnp.mean(after_mix * after_mix, axis=-1, keepdims=True) + 1e-06)
    normed = (after_mix * row_scale * norm_gain).astype(jnp.bfloat16)
    all_rows = collect(normed, "tp", 0)
    gate_all, up_all, down_all = rows_first((gate_weight, up_weight, down_weight), "sp", (0, 0, 1))
    gate = jnp.dot(all_rows, gate_all, preferred_element_type=jnp.float32)
    up = jnp.dot(all_rows, up_all, preferred_element_type=jnp.float32)
    hidden = (jax.nn.silu(gate) * up).astype(jnp.bfloat16)
    picked = hidden
    mixer = sent_and_summed(
        jnp.dot(picked, down_all, preferred_element_type=jnp.float32).astype(jnp.bfloat16), "tp", 0
    )
    return (after_mix + 0.5 * mixer).astype(jnp.bfloat16)


def solution(mesh):
    return jax.shard_map(
        body,
        mesh=mesh,
        in_specs=(
            P(("sp", "tp"), None),
            P("sp", "tp"),
            P("sp", "tp"),
            P("sp", "tp"),
            P("tp"),
            P(),
            P("tp", None),
            P(),
            P("sp", "tp"),
            P("sp", "tp"),
            P("tp", "sp"),
        ),
        out_specs=P(("sp", "tp"), None),
        check_vma=False,
    )
```

profile of v0, /device:TPU:1, one launch (start us, length us, event | category | flops | bytes accessed | tf_op | source)
XLA Modules:
  0.0 425.4 jit_solution(3736161622382868444)
XLA Ops:
  6.5 0.7 all-gather.4.cloned.1.call-update
  7.3 0.7 all-gather.6.cloned.1.call-update
  8.1 1.9 concatenate.3
  10.0 1.1 copy.17
  11.1 89.9 %all-gather.4.cloned.1.call-done = bf16[12288,256]{1,0:T(8,128)(2,1)} async-done(((bf16[384,256]{1,0:T(8,128)(2,1)}), bf16[12288,256]{1,0:T(8,128)(2,1)}) %all-gather.4.cloned.1.call-update) | async-done | bytes 6291472 | tf_op jit(solution)/shard_map/all_gather | solution.py:95
  101.0 21.8 %reshape.51 = bf16[8,1536,2,2,64]{4,3,2,1,0:T(2,128)(2,1)} reshape(bf16[12288,256]{1,0:T(8,128)(2,1)} %all-gather.4.cloned.1.call-done) | data formatting | bytes 12582912 | tf_op jit(solution)/shard_map/reshape | solution.py:105
  122.8 29.8 %copy.19 = bf16[8,1536,2,2,64]{1,4,3,2,0:T(8,128)(2,1)} copy(bf16[8,1536,2,2,64]{4,3,2,1,0:T(2,128)(2,1)} %reshape.51) | data formatting | bytes 12582912
  152.6 36.1 %all-gather.6.cloned.1.call-done = bf16[12288,256]{1,0:T(8,128)(2,1)} async-done(((bf16[384,256]{1,0:T(8,128)(2,1)}), bf16[12288,256]{1,0:T(8,128)(2,1)}) %all-gather.6.cloned.1.call-update) | async-done | bytes 6291472 | tf_op jit(solution)/shard_map/all_gather | solution.py:96
  188.7 9.7 %reshape.52 = bf16[8,1536,2,128]{3,2,1,0:T(2,128)(2,1)} reshape(bf16[12288,256]{1,0:T(8,128)(2,1)} %all-gather.6.cloned.1.call-done) | data formatting | bytes 12582912 | tf_op jit(solution)/shard_map/reshape | solution.py:106
  198.5 128.2 %while.15 = (s32[]{:T(128)}, f32[2,2,384]{2,1,0:T(2,128)S(1)}, f32[2,2,384]{2,1,0:T(2,128)S(1)}, f32[2,2,384,128]{3,2,1,0:T(8,128)S(1)}, bf16[8,1536,2,2,64]{1,4...) while((s32[]{:T(128)}, f32[2,2,384]{2,1,0:T(2,128)S(1)}, ...), condition=%wide.region_3.4_spmd.clone, body=%wide.region_0.3_spmd.clone.sunk | while | flops 925441536 | bytes 71074440 | solution.py:107
  198.5 6.2 %bitcast_reduce_fusion.2 = (f32[2,2,384]{2,1,0:T(2,128)S(1)}, f32[2,2,1536,384]{3,2,1,0:T(8,128)}) fusion(bf16[384,2,2,64]{0,3,2,1:T(8,128)(2,1)S(1)} %get-tuple-element.168, bf16[8,1536,2,2,64]{1,4,3,2,0:T(8,128)(2,1)} %get-tuple-element.167, s32[]{:T(128)} %get-tuple-element.154), kind=kOutput, calls=%fused_computation.1.clone.1 | convolution fusion | flops 306706944 | bytes 10426880 | tf_op jit(solution)/shard_map/while/body/eval_jaxpr/qhcd,khcd->hcqk/dot_general | solution.py:75
  204.7 5.4 %fusion.55 = f32[2,2,384]{2,1,0:T(2,128)S(1)} fusion(f32[2,2,1536,384]{3,2,1,0:T(8,128)} %get-tuple-element.142, f32[2,2,384]{2,1,0:T(2,128)S(1)} %fusion.54), kind=kLoop, calls=%fused_computation.4.clone.1 | loop fusion | flops 7076352 | bytes 9449472 | tf_op jit(solution)/shard_map/while/body/eval_jaxpr/reduce_sum | solution.py:81
  210.2 1.6 constant_dynamic-slice_fusion.2
  211.8 2.6 fusion.57
  214.4 6.2 %bitcast_reduce_fusion.2 = (f32[2,2,384]{2,1,0:T(2,128)S(1)}, f32[2,2,1536,384]{3,2,1,0:T(8,128)}) fusion(bf16[384,2,2,64]{0,3,2,1:T(8,128)(2,1)S(1)} %get-tuple-element.168, bf16[8,1536,2,2,64]{1,4,3,2,0:T(8,128)(2,1)} %get-tuple-element.167, s32[]{:T(128)} %get-tuple-element.154), kind=kOutput, calls=%fused_computation.1.clone.1 | convolution fusion | flops 306706944 | bytes 10426880 | tf_op jit(solution)/shard_map/while/body/eval_jaxpr/qhcd,khcd->hcqk/dot_general | solution.py:75
  220.7 5.4 %fusion.55 = f32[2,2,384]{2,1,0:T(2,128)S(1)} fusion(f32[2,2,1536,384]{3,2,1,0:T(8,128)} %get-tuple-element.142, f32[2,2,384]{2,1,0:T(2,128)S(1)} %fusion.54), kind=kLoop, calls=%fused_computation.4.clone.1 | loop fusion | flops 7076352 | bytes 9449472 | tf_op jit(solution)/shard_map/while/body/eval_jaxpr/reduce_sum | solution.py:81
  226.1 1.6 constant_dynamic-slice_fusion.2
  227.7 2.6 fusion.57
  230.4 6.2 %bitcast_reduce_fusion.2 = (f32[2,2,384]{2,1,0:T(2,128)S(1)}, f32[2,2,1536,384]{3,2,1,0:T(8,128)}) fusion(bf16[384,2,2,64]{0,3,2,1:T(8,128)(2,1)S(1)} %get-tuple-element.168, bf16[8,1536,2,2,64]{1,4,3,2,0:T(8,128)(2,1)} %get-tuple-element.167, s32[]{:T(128)} %get-tuple-element.154), kind=kOutput, calls=%fused_computation.1.clone.1 | convolution fusion | flops 306706944 | bytes 10426880 | tf_op jit(solution)/shard_map/while/body/eval_jaxpr/qhcd,khcd->hcqk/dot_general | solution.py:75
  236.6 5.6 %fusion.55 = f32[2,2,384]{2,1,0:T(2,128)S(1)} fusion(f32[2,2,1536,384]{3,2,1,0:T(8,128)} %get-tuple-element.142, f32[2,2,384]{2,1,0:T(2,128)S(1)} %fusion.54), kind=kLoop, calls=%fused_computation.4.clone.1 | loop fusion | flops 7076352 | bytes 9449472 | tf_op jit(solution)/shard_map/while/body/eval_jaxpr/reduce_sum | solution.py:81
  242.2 1.9 constant_dynamic-slice_fusion.2
  244.1 2.6 fusion.57
  246.8 6.2 %bitcast_reduce_fusion.2 = (f32[2,2,384]{2,1,0:T(2,128)S(1)}, f32[2,2,1536,384]{3,2,1,0:T(8,128)}) fusion(bf16[384,2,2,64]{0,3,2,1:T(8,128)(2,1)S(1)} %get-tuple-element.168, bf16[8,1536,2,2,64]{1,4,3,2,0:T(8,128)(2,1)} %get-tuple-element.167, s32[]{:T(128)} %get-tuple-element.154), kind=kOutput, calls=%fused_computation.1.clone.1 | convolution fusion | flops 306706944 | bytes 10426880 | tf_op jit(solution)/shard_map/while/body/eval_jaxpr/qhcd,khcd->hcqk/dot_general | solution.py:75
  253.0 5.6 %fusion.55 = f32[2,2,384]{2,1,0:T(2,128)S(1)} fusion(f32[2,2,1536,384]{3,2,1,0:T(8,128)} %get-tuple-element.142, f32[2,2,384]{2,1,0:T(2,128)S(1)} %fusion.54), kind=kLoop, calls=%fused_computation.4.clone.1 | loop fusion | flops 7076352 | bytes 9449472 | tf_op jit(solution)/shard_map/while/body/eval_jaxpr/reduce_sum | solution.py:81
  258.7 1.6 constant_dynamic-slice_fusion.2
  260.3 2.6 fusion.57
  263.0 6.2 %bitcast_reduce_fusion.2 = (f32[2,2,384]{2,1,0:T(2,128)S(1)}, f32[2,2,1536,384]{3,2,1,0:T(8,128)}) fusion(bf16[384,2,2,64]{0,3,2,1:T(8,128)(2,1)S(1)} %get-tuple-element.168, bf16[8,1536,2,2,64]{1,4,3,2,0:T(8,128)(2,1)} %get-tuple-element.167, s32[]{:T(128)} %get-tuple-element.154), kind=kOutput, calls=%fused_computation.1.clone.1 | convolution fusion | flops 306706944 | bytes 10426880 | tf_op jit(solution)/shard_map/while/body/eval_jaxpr/qhcd,khcd->hcqk/dot_general | solution.py:75
  269.2 5.4 %fusion.55 = f32[2,2,384]{2,1,0:T(2,128)S(1)} fusion(f32[2,2,1536,384]{3,2,1,0:T(8,128)} %get-tuple-element.142, f32[2,2,384]{2,1,0:T(2,128)S(1)} %fusion.54), kind=kLoop, calls=%fused_computation.4.clone.1 | loop fusion | flops 7076352 | bytes 9449472 | tf_op jit(solution)/shard_map/while/body/eval_jaxpr/reduce_sum | solution.py:81
  274.7 1.6 constant_dynamic-slice_fusion.2
  276.3 2.6 fusion.57
  279.0 6.2 %bitcast_reduce_fusion.2 = (f32[2,2,384]{2,1,0:T(2,128)S(1)}, f32[2,2,1536,384]{3,2,1,0:T(8,128)}) fusion(bf16[384,2,2,64]{0,3,2,1:T(8,128)(2,1)S(1)} %get-tuple-element.168, bf16[8,1536,2,2,64]{1,4,3,2,0:T(8,128)(2,1)} %get-tuple-element.167, s32[]{:T(128)} %get-tuple-element.154), kind=kOutput, calls=%fused_computation.1.clone.1 | convolution fusion | flops 306706944 | bytes 10426880 | tf_op jit(solution)/shard_map/while/body/eval_jaxpr/qhcd,khcd->hcqk/dot_general | solution.py:75
  285.2 5.4 %fusion.55 = f32[2,2,384]{2,1,0:T(2,128)S(1)} fusion(f32[2,2,1536,384]{3,2,1,0:T(8,128)} %get-tuple-element.142, f32[2,2,384]{2,1,0:T(2,128)S(1)} %fusion.54), kind=kLoop, calls=%fused_computation.4.clone.1 | loop fusion | flops 7076352 | bytes 9449472 | tf_op jit(solution)/shard_map/while/body/eval_jaxpr/reduce_sum | solution.py:81
  290.6 1.6 constant_dynamic-slice_fusion.2
  292.2 2.6 fusion.57
  294.9 6.2 %bitcast_reduce_fusion.2 = (f32[2,2,384]{2,1,0:T(2,128)S(1)}, f32[2,2,1536,384]{3,2,1,0:T(8,128)}) fusion(bf16[384,2,2,64]{0,3,2,1:T(8,128)(2,1)S(1)} %get-tuple-element.168, bf16[8,1536,2,2,64]{1,4,3,2,0:T(8,128)(2,1)} %get-tuple-element.167, s32[]{:T(128)} %get-tuple-element.154), kind=kOutput, calls=%fused_computation.1.clone.1 | convolution fusion | flops 306706944 | bytes 10426880 | tf_op jit(solution)/shard_map/while/body/eval_jaxpr/qhcd,khcd->hcqk/dot_general | solution.py:75
  301.1 5.4 %fusion.55 = f32[2,2,384]{2,1,0:T(2,128)S(1)} fusion(f32[2,2,1536,384]{3,2,1,0:T(8,128)} %get-tuple-element.142, f32[2,2,384]{2,1,0:T(2,128)S(1)} %fusion.54), kind=kLoop, calls=%fused_computation.4.clone.1 | loop fusion | flops 7076352 | bytes 9449472 | tf_op jit(solution)/shard_map/while/body/eval_jaxpr/reduce_sum | solution.py:81
  306.5 1.6 constant_dynamic-slice_fusion.2
  308.1 2.6 fusion.57
  310.8 6.2 %bitcast_reduce_fusion.2 = (f32[2,2,384]{2,1,0:T(2,128)S(1)}, f32[2,2,1536,384]{3,2,1,0:T(8,128)}) fusion(bf16[384,2,2,64]{0,3,2,1:T(8,128)(2,1)S(1)} %get-tuple-element.168, bf16[8,1536,2,2,64]{1,4,3,2,0:T(8,128)(2,1)} %get-tuple-element.167, s32[]{:T(128)} %get-tuple-element.154), kind=kOutput, calls=%fused_computation.1.clone.1 | convolution fusion | flops 306706944 | bytes 10426880 | tf_op jit(solution)/shard_map/while/body/eval_jaxpr/qhcd,khcd->hcqk/dot_general | solution.py:75
  317.0 5.4 %fusion.55 = f32[2,2,384]{2,1,0:T(2,128)S(1)} fusion(f32[2,2,1536,384]{3,2,1,0:T(8,128)} %get-tuple-element.142, f32[2,2,384]{2,1,0:T(2,128)S(1)} %fusion.54), kind=kLoop, calls=%fused_computation.4.clone.1 | loop fusion | flops 7076352 | bytes 9449472 | tf_op jit(solution)/shard_map/while/body/eval_jaxpr/reduce_sum | solution.py:81
  322.4 1.6 constant_dynamic-slice_fusion.2
  324.0 2.6 fusion.57
  328.3 26.4 %all_to_all.15 = bf16[8,48,2048]{2,1,0:T(8,128)(2,1)S(1)} all-to-all(bf16[8,48,2048]{2,1,0:T(8,128)(2,1)S(1)} %bitcast.67), channel_id=1, replica_groups=mesh['sp'=32,'tp'=8] {'tp'}, dimensions={0} | all-to-all | bytes 3145728 | tf_op jit(solution)/shard_map/all_to_all | solution.py:19
  355.4 24.0 %all_to_all.16 = bf16[8,48,2048]{2,1,0:T(8,128)(2,1)S(1)} all-to-all(bf16[8,48,2048]{2,1,0:T(8,128)(2,1)S(1)} %broadcast_in_dim.13), channel_id=1, replica_groups=mesh['sp'=32,'tp'=8] {'tp'}, dimensions={0} | all-to-all | bytes 3145728 | tf_op jit(solution)/shard_map/all_to_all | solution.py:25
  379.5 4.6 %fusion.21 = f32[384,704]{0,1:T(8,128)} fusion(bf16[384,2048]{1,0:T(8,128)(2,1)S(1)} %bitcast.68, bf16[2048,2112]{1,0:T(8,128)(2,1)} %all-gather.8.cloned.1.call-done), kind=kOutput, calls=%fused_computation.26 | convolution fusion | flops 1107296256 | bytes 5799936 | tf_op jit(solution)/shard_map/dot_general | solution.py:125
  384.0 8.8 %fusion.23 = bf16[384,2048]{1,0:T(8,128)(2,1)} fusion(bf16[2048,2112]{1,0:T(8,128)(2,1)} %all-gather.8.cloned.1.call-done, bf16[384,2048]{1,0:T(8,128)(2,1)S(1)} %bitcast.69, f32[384,704]{0,1:T(8,128)} %fusion.21), kind=kOutput, calls=%fused_computation.30 | convolution fusion | flops 2217000960 | bytes 10518528 | tf_op jit(solution)/shard_map/dot_general | solution.py:130
  392.8 25.1 %all_to_all.17 = bf16[8,48,2048]{2,1,0:T(8,128)(2,1)S(1)} all-to-all(bf16[8,48,2048]{2,1,0:T(8,128)(2,1)} %bitcast.70), channel_id=1, replica_groups=mesh['sp'=32,'tp'=8] {'tp'}, dimensions={0} | all-to-all | bytes 3145728 | tf_op jit(solution)/shard_map/all_to_all | solution.py:19
  418.1 0.8 add_convert_fusion
  (71 shorter events, 2.8 us)
Async XLA Ops:
  6.5 321.1 %copy-start = (bf16[256,2048]{1,0:T(8,128)(2,1)S(1)}, bf16[256,2048]{1,0:T(8,128)(2,1)}, u32[]{:S(2)}) copy-start(bf16[256,2048]{1,0:T(8,128)(2,1)} %param.19) | copy-start | bytes 3145732
  6.5 94.5 %all-gather.4.cloned.1.call-start = ((), (), s32[]{:S(2)}) async-start(), calls=%async_computation.3 | async-start | bytes 6488064 | tf_op jit(solution)/shard_map/all_gather | solution.py:95
  7.3 181.5 %all-gather.6.cloned.1.call-start = ((), (), s32[]{:S(2)}) async-start(), calls=%async_computation.4 | async-start | bytes 6488064 | tf_op jit(solution)/shard_map/all_gather | solution.py:96
  8.0 371.5 %all-gather.8.cloned.1.call-start = ((), (), s32[]{:S(2)}) async-start(), calls=%async_computation.5 | async-start | bytes 9191424 | tf_op jit(solution)/shard_map/all_gather | solution.py:43
  204.7 7.1 %copy-start.1 = (f32[2,2,1536,384]{3,2,1,0:T(8,128)S(1)}, f32[2,2,1536,384]{3,2,1,0:T(8,128)}, u32[]{:S(2)}) copy-start(f32[2,2,1536,384]{3,2,1,0:T(8,128)} %get-tuple-element.142) | copy-start | bytes 28311556 | tf_op jit(solution)/shard_map/while
  220.7 7.1 %copy-start.1 = (f32[2,2,1536,384]{3,2,1,0:T(8,128)S(1)}, f32[2,2,1536,384]{3,2,1,0:T(8,128)}, u32[]{:S(2)}) copy-start(f32[2,2,1536,384]{3,2,1,0:T(8,128)} %get-tuple-element.142) | copy-start | bytes 28311556 | tf_op jit(solution)/shard_map/while
  236.6 7.5 %copy-start.1 = (f32[2,2,1536,384]{3,2,1,0:T(8,128)S(1)}, f32[2,2,1536,384]{3,2,1,0:T(8,128)}, u32[]{:S(2)}) copy-start(f32[2,2,1536,384]{3,2,1,0:T(8,128)} %get-tuple-element.142) | copy-start | bytes 28311556 | tf_op jit(solution)/shard_map/while
  253.0 7.3 %copy-start.1 = (f32[2,2,1536,384]{3,2,1,0:T(8,128)S(1)}, f32[2,2,1536,384]{3,2,1,0:T(8,128)}, u32[]{:S(2)}) copy-start(f32[2,2,1536,384]{3,2,1,0:T(8,128)} %get-tuple-element.142) | copy-start | bytes 28311556 | tf_op jit(solution)/shard_map/while
  269.2 7.1 %copy-start.1 = (f32[2,2,1536,384]{3,2,1,0:T(8,128)S(1)}, f32[2,2,1536,384]{3,2,1,0:T(8,128)}, u32[]{:S(2)}) copy-start(f32[2,2,1536,384]{3,2,1,0:T(8,128)} %get-tuple-element.142) | copy-start | bytes 28311556 | tf_op jit(solution)/shard_map/while
  285.2 7.0 %copy-start.1 = (f32[2,2,1536,384]{3,2,1,0:T(8,128)S(1)}, f32[2,2,1536,384]{3,2,1,0:T(8,128)}, u32[]{:S(2)}) copy-start(f32[2,2,1536,384]{3,2,1,0:T(8,128)} %get-tuple-element.142) | copy-start | bytes 28311556 | tf_op jit(solution)/shard_map/while
  301.1 7.0 %copy-start.1 = (f32[2,2,1536,384]{3,2,1,0:T(8,128)S(1)}, f32[2,2,1536,384]{3,2,1,0:T(8,128)}, u32[]{:S(2)}) copy-start(f32[2,2,1536,384]{3,2,1,0:T(8,128)} %get-tuple-element.142) | copy-start | bytes 28311556 | tf_op jit(solution)/shard_map/while
  317.0 7.0 %copy-start.1 = (f32[2,2,1536,384]{3,2,1,0:T(8,128)S(1)}, f32[2,2,1536,384]{3,2,1,0:T(8,128)}, u32[]{:S(2)}) copy-start(f32[2,2,1536,384]{3,2,1,0:T(8,128)} %get-tuple-element.142) | copy-start | bytes 28311556 | tf_op jit(solution)/shard_map/while
  326.7 0.7 copy-start.4
  326.7 0.8 copy-start.5
  328.3 26.7 %copy-start.2 = (bf16[48,2048]{1,0:T(8,128)(2,1)S(1)}, bf16[48,2048]{1,0:T(8,128)(2,1)}, u32[]{:S(2)}) copy-start(bf16[48,2048]{1,0:T(8,128)(2,1)} %param.13) | copy-start | bytes 589828
  328.3 26.8 %copy-start.3 = (f32[2048]{0:T(1024)S(1)}, f32[2048]{0:T(1024)}, u32[]{:S(2)}) copy-start(f32[2048]{0:T(1024)} %param.20) | copy-start | bytes 24580
Sparse Core Ops, SparseCore 0:
  9.9 91.0 all-gather.3
  103.6 85.0 all-gather.5
  191.3 97.5 all-gather.7
where the time goes:
time: 428 us; the launch traced here: 425 us
  waiting for transfers between devices  127 us (30%)
  matrix products  84.7 us (20%)
  local copies, waits for them, and re-layouts  78.1 us (18%)
  blocking collectives  75.5 us (18%)
  other arithmetic  45.7 us (11%)
  between operations  13.3 us (3%)
    all_gather x1, waiting for transfers between devices, body(): key_piece = lax.all_gather(keys, 'sp', axis=0, tiled=True)  89.9 us
    all_to_all x2, blocking collectives, sent_and_summed(): lax.all_to_all(parts, axis, split_axis=0, concat_axis=0, tiled=True)  51.5 us
    dot_general x8, matrix products, one_block(): jnp.einsum('qhcd,khcd->hcqk', query_four, key_block, preferred_element_ty...  49.6 us
    reduce_sum x8, other arithmetic, one_block(): total = total * rescale + jnp.sum(expo, axis=-1)  43.7 us
    all_gather x1, waiting for transfers between devices, body(): value_piece = lax.all_gather(values, 'sp', axis=0, tiled=True)  36.1 us
    unnamed x12, local copies, waits for them, and re-layouts  31.2 us
    all_to_all x1, blocking collectives, sent_to_all(): return lax.all_to_all(copies, axis, split_axis=0, concat_axis=0, tiled=True)  24 us
    reshape x1, local copies, waits for them, and re-layouts, body(): key_blocks = key_piece.reshape(blocks, width, heads_local, 2, DH)  21.8 us
  transfers between devices with their start and end apart: 3, of which 2 were waited for; matrix products, arithmetic and copies ran while one was open for 46% of the time, Pallas kernels for 0%

commit v1 on v0

--- a/solution.py
+++ b/solution.py
@@ -92,7 +92,9 @@
         jnp.zeros((heads_local, 2, tok_local), jnp.float32),
         jnp.zeros((heads_local, 2, tok_local, VD), jnp.float32),
     )
-    key_piece = lax.all_gather(keys, "sp", axis=0, tiled=True)
+    key_piece = jnp.concatenate(
+        lax.all_to_all(jnp.stack([keys] * lax.axis_size("sp")), "sp", 0, 0), axis=0
+    )
     value_piece = lax.all_gather(values, "sp", axis=0, tiled=True)
     count = key_piece.shape[0]
     shards = max(count // tok_local, 1)

time: 428 us -> 465 us (1.086)
  waiting for transfers between devices: 127 us -> 173 us
  local copies, waits for them, and re-layouts: 78.1 us -> 56.6 us
  starting transfers between devices: 0.08 us -> 12.3 us
    all_to_all x0 -> x1, waiting for transfers between devices: none -> 173 us  [body(): lax.all_to_all(jnp.stack([keys] * lax.axis_size('sp')), 'sp', 0, 0)]
    all_gather x1 -> x0, waiting for transfers between devices: 89.9 us -> none  [body(): key_piece = lax.all_gather(keys, 'sp', axis=0, tiled=True)]
    all_gather x1, waiting for transfers between devices: 36.1 us -> 0.01 us  [body(): value_piece = lax.all_gather(values, 'sp', axis=0, tiled=True)]
    unnamed x12 -> x21, local copies, waits for them, and re-layouts: 31.2 us -> 9.01 us
    reshape x1 -> x0, local copies, waits for them, and re-layouts: 21.8 us -> none  [body(): key_blocks = key_piece.reshape(blocks, width, heads_local, 2, DH)]
    another operation x0 -> x2, local copies, waits for them, and re-layouts: none -> 14.4 us  [the longest x1 10.7 us: body(): key_blocks = key_piece.reshape(blocks, width, heads_local, 2, DH)]
    all_to_all x0 -> x1, starting transfers between devices: none -> 12.3 us  [body(): lax.all_to_all(jnp.stack([keys] * lax.axis_size('sp')), 'sp', 0, 0)]
    all_to_all x0 -> x1, local copies, waits for them, and re-layouts: none -> 9.22 us  [body(): lax.all_to_all(jnp.stack([keys] * lax.axis_size('sp')), 'sp', 0, 0)]
  transfers between devices with their start and end apart: 3 -> 3, of which waited for: 2 -> 1; matrix products, arithmetic and copies ran while one was open for 46% -> 37% of each run, Pallas kernels for 0% -> 0%
where the time goes in v1:
time: 465 us; the launch traced here: 464 us
  waiting for transfers between devices  173 us (37%)
  matrix products  84.6 us (18%)
  blocking collectives  77 us (17%)
  local copies, waits for them, and re-layouts  56.6 us (12%)
  other arithmetic  45.6 us (10%)
  between operations  13.6 us (3%)
  starting transfers between devices  12.3 us (3%)
    all_to_all x1, waiting for transfers between devices, body(): lax.all_to_all(jnp.stack([keys] * lax.axis_size('sp')), 'sp', 0, 0)  173 us
    all_to_all x2, blocking collectives, sent_and_summed(): lax.all_to_all(parts, axis, split_axis=0, concat_axis=0, tiled=True)  53 us
    dot_general x8, matrix products, one_block(): jnp.einsum('qhcd,khcd->hcqk', query_four, key_block, preferred_element_ty...  49.6 us
    reduce_sum x8, other arithmetic, one_block(): total = total * rescale + jnp.sum(expo, axis=-1)  43.5 us
    all_to_all x1, blocking collectives, sent_to_all(): return lax.all_to_all(copies, axis, split_axis=0, concat_axis=0, tiled=True)  24 us
    dot_general x8, matrix products, one_block(): jnp.einsum('hcqk,khe->hcqe', expo.astype(jnp.bfloat16), value_block, pref...  21.2 us
    dynamic_slice x8, local copies, waits for them, and re-layouts, body(): state, unused = lax.scan(one_block, start_state, (key_blocks, value_blocks))  12.9 us
    all_to_all x1, starting transfers between devices, body(): lax.all_to_all(jnp.stack([keys] * lax.axis_size('sp')), 'sp', 0, 0)  12.3 us
  transfers between devices with their start and end apart: 3, of which 1 were waited for; matrix products, arithmetic and copies ran while one was open for 37% of the time, Pallas kernels for 0%

profile of v1, /device:TPU:1, one launch (start us, length us, event | category | flops | bytes accessed | tf_op | source)
XLA Modules:
  0.0 463.6 jit_solution(5589878337944765438)
XLA Ops:
  7.3 1.1 copy.24
  8.4 3.7 stack.2
  12.0 12.3 %all-to-all-start = ((bf16[32,384,256]{1,2,0:T(8,128)(2,1)}), bf16[32,384,256]{1,2,0:T(8,128)(2,1)}, u32[]{:S(2)}, u32[]{:S(2)}) async-start(bf16[32,384,256]{1,2,0:T(8,128)(2,1)} %stack.2), calls=%async_computation | async-start | bytes 12582912 | tf_op jit(solution)/shard_map/all_to_all | solution.py:96
  24.4 0.8 concatenate.3
  25.5 172.5 %all-to-all-done = bf16[32,384,256]{1,2,0:T(8,128)(2,1)} async-done(((bf16[32,384,256]{1,2,0:T(8,128)(2,1)}), bf16[32,384,256]{1,2,0:T(8,128)(2,1)}, u32[]{:S(2)}, u32[]{:S(2)}) %all-to-all-start) | async-done | bytes 6291488 | tf_op jit(solution)/shard_map/all_to_all | solution.py:96
  198.0 9.2 %copy.25 = bf16[32,384,256]{1,0,2:T(8,128)(2,1)} copy(bf16[32,384,256]{1,2,0:T(8,128)(2,1)} %all-to-all-done) | data formatting | bytes 12582912 | tf_op jit(solution)/shard_map/all_to_all | solution.py:96
  207.2 10.7 %reshape_reshape.3 = bf16[8,1536,2,2,64]{1,0,4,3,2:T(8,128)(2,1)} reshape(bf16[32,384,256]{1,0,2:T(8,128)(2,1)} %copy.25) | data formatting | bytes 12582912 | tf_op jit(solution)/shard_map/reshape;reshape | solution.py:107
  217.9 7.4 %copy.28 = bf16[8,1536,2,2,64]{1,4,3,2,0:T(8,128)(2,1)} copy(bf16[8,1536,2,2,64]{1,0,4,3,2:T(8,128)(2,1)} %reshape_reshape.3) | data formatting | bytes 12582912
  225.4 9.8 %reshape.49 = bf16[8,1536,2,128]{3,2,1,0:T(2,128)(2,1)} reshape(bf16[12288,256]{1,0:T(8,128)(2,1)} %all-gather.3.cloned.1.call-done) | data formatting | bytes 12582912 | tf_op jit(solution)/shard_map/reshape | solution.py:108
  235.1 128.0 %while.15 = (s32[]{:T(128)}, f32[2,2,384]{2,1,0:T(2,128)S(1)}, f32[2,2,384]{2,1,0:T(2,128)S(1)}, f32[2,2,384,128]{3,2,1,0:T(8,128)S(1)}, bf16[8,1536,2,2,64]{1,4...) while((s32[]{:T(128)}, f32[2,2,384]{2,1,0:T(2,128)S(1)}, ...), condition=%wide.region_3.4_spmd.clone, body=%wide.region_0.3_spmd.clone.sunk | while | flops 925441536 | bytes 71074440 | solution.py:109
  235.1 6.2 %bitcast_reduce_fusion.2 = (f32[2,2,384]{2,1,0:T(2,128)S(1)}, f32[2,2,1536,384]{3,2,1,0:T(8,128)}) fusion(bf16[384,2,2,64]{0,3,2,1:T(8,128)(2,1)S(1)} %get-tuple-element.175, bf16[8,1536,2,2,64]{1,4,3,2,0:T(8,128)(2,1)} %get-tuple-element.174, s32[]{:T(128)} %get-tuple-element.161), kind=kOutput, calls=%fused_computation.1.clone.1 | convolution fusion | flops 306706944 | bytes 10426880 | tf_op jit(solution)/shard_map/while/body/eval_jaxpr/qhcd,khcd->hcqk/dot_general | solution.py:75
  241.4 5.4 %fusion.55 = f32[2,2,384]{2,1,0:T(2,128)S(1)} fusion(f32[2,2,1536,384]{3,2,1,0:T(8,128)} %get-tuple-element.149, f32[2,2,384]{2,1,0:T(2,128)S(1)} %fusion.54), kind=kLoop, calls=%fused_computation.4.clone.1 | loop fusion | flops 7076352 | bytes 9449472 | tf_op jit(solution)/shard_map/while/body/eval_jaxpr/reduce_sum | solution.py:81
  246.8 1.6 constant_dynamic-slice_fusion.2
  248.4 2.6 fusion.57
  251.0 6.2 %bitcast_reduce_fusion.2 = (f32[2,2,384]{2,1,0:T(2,128)S(1)}, f32[2,2,1536,384]{3,2,1,0:T(8,128)}) fusion(bf16[384,2,2,64]{0,3,2,1:T(8,128)(2,1)S(1)} %get-tuple-element.175, bf16[8,1536,2,2,64]{1,4,3,2,0:T(8,128)(2,1)} %get-tuple-element.174, s32[]{:T(128)} %get-tuple-element.161), kind=kOutput, calls=%fused_computation.1.clone.1 | convolution fusion | flops 306706944 | bytes 10426880 | tf_op jit(solution)/shard_map/while/body/eval_jaxpr/qhcd,khcd->hcqk/dot_general | solution.py:75
  257.3 5.5 %fusion.55 = f32[2,2,384]{2,1,0:T(2,128)S(1)} fusion(f32[2,2,1536,384]{3,2,1,0:T(8,128)} %get-tuple-element.149, f32[2,2,384]{2,1,0:T(2,128)S(1)} %fusion.54), kind=kLoop, calls=%fused_computation.4.clone.1 | loop fusion | flops 7076352 | bytes 9449472 | tf_op jit(solution)/shard_map/while/body/eval_jaxpr/reduce_sum | solution.py:81
  262.8 1.7 constant_dynamic-slice_fusion.2
  264.5 2.6 fusion.57
  267.1 6.2 %bitcast_reduce_fusion.2 = (f32[2,2,384]{2,1,0:T(2,128)S(1)}, f32[2,2,1536,384]{3,2,1,0:T(8,128)}) fusion(bf16[384,2,2,64]{0,3,2,1:T(8,128)(2,1)S(1)} %get-tuple-element.175, bf16[8,1536,2,2,64]{1,4,3,2,0:T(8,128)(2,1)} %get-tuple-element.174, s32[]{:T(128)} %get-tuple-element.161), kind=kOutput, calls=%fused_computation.1.clone.1 | convolution fusion | flops 306706944 | bytes 10426880 | tf_op jit(solution)/shard_map/while/body/eval_jaxpr/qhcd,khcd->hcqk/dot_general | solution.py:75
  273.4 5.7 %fusion.55 = f32[2,2,384]{2,1,0:T(2,128)S(1)} fusion(f32[2,2,1536,384]{3,2,1,0:T(8,128)} %get-tuple-element.149, f32[2,2,384]{2,1,0:T(2,128)S(1)} %fusion.54), kind=kLoop, calls=%fused_computation.4.clone.1 | loop fusion | flops 7076352 | bytes 9449472 | tf_op jit(solution)/shard_map/while/body/eval_jaxpr/reduce_sum | solution.py:81
  279.1 1.7 constant_dynamic-slice_fusion.2
  280.8 2.6 fusion.57
  283.5 6.2 %bitcast_reduce_fusion.2 = (f32[2,2,384]{2,1,0:T(2,128)S(1)}, f32[2,2,1536,384]{3,2,1,0:T(8,128)}) fusion(bf16[384,2,2,64]{0,3,2,1:T(8,128)(2,1)S(1)} %get-tuple-element.175, bf16[8,1536,2,2,64]{1,4,3,2,0:T(8,128)(2,1)} %get-tuple-element.174, s32[]{:T(128)} %get-tuple-element.161), kind=kOutput, calls=%fused_computation.1.clone.1 | convolution fusion | flops 306706944 | bytes 10426880 | tf_op jit(solution)/shard_map/while/body/eval_jaxpr/qhcd,khcd->hcqk/dot_general | solution.py:75
  289.7 5.4 %fusion.55 = f32[2,2,384]{2,1,0:T(2,128)S(1)} fusion(f32[2,2,1536,384]{3,2,1,0:T(8,128)} %get-tuple-element.149, f32[2,2,384]{2,1,0:T(2,128)S(1)} %fusion.54), kind=kLoop, calls=%fused_computation.4.clone.1 | loop fusion | flops 7076352 | bytes 9449472 | tf_op jit(solution)/shard_map/while/body/eval_jaxpr/reduce_sum | solution.py:81
  295.1 1.7 constant_dynamic-slice_fusion.2
  296.8 2.6 fusion.57
  299.5 6.2 %bitcast_reduce_fusion.2 = (f32[2,2,384]{2,1,0:T(2,128)S(1)}, f32[2,2,1536,384]{3,2,1,0:T(8,128)}) fusion(bf16[384,2,2,64]{0,3,2,1:T(8,128)(2,1)S(1)} %get-tuple-element.175, bf16[8,1536,2,2,64]{1,4,3,2,0:T(8,128)(2,1)} %get-tuple-element.174, s32[]{:T(128)} %get-tuple-element.161), kind=kOutput, calls=%fused_computation.1.clone.1 | convolution fusion | flops 306706944 | bytes 10426880 | tf_op jit(solution)/shard_map/while/body/eval_jaxpr/qhcd,khcd->hcqk/dot_general | solution.py:75
  305.7 5.4 %fusion.55 = f32[2,2,384]{2,1,0:T(2,128)S(1)} fusion(f32[2,2,1536,384]{3,2,1,0:T(8,128)} %get-tuple-element.149, f32[2,2,384]{2,1,0:T(2,128)S(1)} %fusion.54), kind=kLoop, calls=%fused_computation.4.clone.1 | loop fusion | flops 7076352 | bytes 9449472 | tf_op jit(solution)/shard_map/while/body/eval_jaxpr/reduce_sum | solution.py:81
  311.1 1.6 constant_dynamic-slice_fusion.2
  312.7 2.6 fusion.57
  315.4 6.2 %bitcast_reduce_fusion.2 = (f32[2,2,384]{2,1,0:T(2,128)S(1)}, f32[2,2,1536,384]{3,2,1,0:T(8,128)}) fusion(bf16[384,2,2,64]{0,3,2,1:T(8,128)(2,1)S(1)} %get-tuple-element.175, bf16[8,1536,2,2,64]{1,4,3,2,0:T(8,128)(2,1)} %get-tuple-element.174, s32[]{:T(128)} %get-tuple-element.161), kind=kOutput, calls=%fused_computation.1.clone.1 | convolution fusion | flops 306706944 | bytes 10426880 | tf_op jit(solution)/shard_map/while/body/eval_jaxpr/qhcd,khcd->hcqk/dot_general | solution.py:75
  321.6 5.4 %fusion.55 = f32[2,2,384]{2,1,0:T(2,128)S(1)} fusion(f32[2,2,1536,384]{3,2,1,0:T(8,128)} %get-tuple-element.149, f32[2,2,384]{2,1,0:T(2,128)S(1)} %fusion.54), kind=kLoop, calls=%fused_computation.4.clone.1 | loop fusion | flops 7076352 | bytes 9449472 | tf_op jit(solution)/shard_map/while/body/eval_jaxpr/reduce_sum | solution.py:81
  327.0 1.6 constant_dynamic-slice_fusion.2
  328.6 2.6 fusion.57
  331.3 6.2 %bitcast_reduce_fusion.2 = (f32[2,2,384]{2,1,0:T(2,128)S(1)}, f32[2,2,1536,384]{3,2,1,0:T(8,128)}) fusion(bf16[384,2,2,64]{0,3,2,1:T(8,128)(2,1)S(1)} %get-tuple-element.175, bf16[8,1536,2,2,64]{1,4,3,2,0:T(8,128)(2,1)} %get-tuple-element.174, s32[]{:T(128)} %get-tuple-element.161), kind=kOutput, calls=%fused_computation.1.clone.1 | convolution fusion | flops 306706944 | bytes 10426880 | tf_op jit(solution)/shard_map/while/body/eval_jaxpr/qhcd,khcd->hcqk/dot_general | solution.py:75
  337.5 5.4 %fusion.55 = f32[2,2,384]{2,1,0:T(2,128)S(1)} fusion(f32[2,2,1536,384]{3,2,1,0:T(8,128)} %get-tuple-element.149, f32[2,2,384]{2,1,0:T(2,128)S(1)} %fusion.54), kind=kLoop, calls=%fused_computation.4.clone.1 | loop fusion | flops 7076352 | bytes 9449472 | tf_op jit(solution)/shard_map/while/body/eval_jaxpr/reduce_sum | solution.py:81
  342.9 1.6 constant_dynamic-slice_fusion.2
  344.5 2.6 fusion.57
  347.2 6.2 %bitcast_reduce_fusion.2 = (f32[2,2,384]{2,1,0:T(2,128)S(1)}, f32[2,2,1536,384]{3,2,1,0:T(8,128)}) fusion(bf16[384,2,2,64]{0,3,2,1:T(8,128)(2,1)S(1)} %get-tuple-element.175, bf16[8,1536,2,2,64]{1,4,3,2,0:T(8,128)(2,1)} %get-tuple-element.174, s32[]{:T(128)} %get-tuple-element.161), kind=kOutput, calls=%fused_computation.1.clone.1 | convolution fusion | flops 306706944 | bytes 10426880 | tf_op jit(solution)/shard_map/while/body/eval_jaxpr/qhcd,khcd->hcqk/dot_general | solution.py:75
  353.4 5.4 %fusion.55 = f32[2,2,384]{2,1,0:T(2,128)S(1)} fusion(f32[2,2,1536,384]{3,2,1,0:T(8,128)} %get-tuple-element.149, f32[2,2,384]{2,1,0:T(2,128)S(1)} %fusion.54), kind=kLoop, calls=%fused_computation.4.clone.1 | loop fusion | flops 7076352 | bytes 9449472 | tf_op jit(solution)/shard_map/while/body/eval_jaxpr/reduce_sum | solution.py:81
  358.8 1.6 constant_dynamic-slice_fusion.2
  360.4 2.6 fusion.57
  364.7 27.9 %all_to_all.20 = bf16[8,48,2048]{2,1,0:T(8,128)(2,1)S(1)} all-to-all(bf16[8,48,2048]{2,1,0:T(8,128)(2,1)S(1)} %bitcast.69), channel_id=1, replica_groups=mesh['sp'=32,'tp'=8] {'tp'}, dimensions={0} | all-to-all | bytes 3145728 | tf_op jit(solution)/shard_map/all_to_all | solution.py:19
  393.3 24.0 %all_to_all.21 = bf16[8,48,2048]{2,1,0:T(8,128)(2,1)S(1)} all-to-all(bf16[8,48,2048]{2,1,0:T(8,128)(2,1)S(1)} %broadcast_in_dim.13), channel_id=1, replica_groups=mesh['sp'=32,'tp'=8] {'tp'}, dimensions={0} | all-to-all | bytes 3145728 | tf_op jit(solution)/shard_map/all_to_all | solution.py:25
  417.3 4.6 fusion.21
  421.9 8.7 %fusion.23 = bf16[384,2048]{1,0:T(8,128)(2,1)} fusion(bf16[2048,2112]{1,0:T(8,128)(2,1)} %all-gather.5.cloned.1.call-done, bf16[384,2048]{1,0:T(8,128)(2,1)S(1)} %bitcast.71, f32[384,704]{0,1:T(8,128)} %fusion.21), kind=kOutput, calls=%fused_computation.30 | convolution fusion | flops 2217000960 | bytes 10518528 | tf_op jit(solution)/shard_map/dot_general | solution.py:132
  430.7 25.1 %all_to_all.22 = bf16[8,48,2048]{2,1,0:T(8,128)(2,1)S(1)} all-to-all(bf16[8,48,2048]{2,1,0:T(8,128)(2,1)} %bitcast.72), channel_id=1, replica_groups=mesh['sp'=32,'tp'=8] {'tp'}, dimensions={0} | all-to-all | bytes 3145728 | tf_op jit(solution)/shard_map/all_to_all | solution.py:19
  456.0 0.8 add_convert_fusion
  (81 shorter events, 3.7 us)
Async XLA Ops:
  6.5 357.5 %copy-start = (bf16[256,2048]{1,0:T(8,128)(2,1)S(1)}, bf16[256,2048]{1,0:T(8,128)(2,1)}, u32[]{:S(2)}) copy-start(bf16[256,2048]{1,0:T(8,128)(2,1)} %param.19) | copy-start | bytes 3145732
  6.5 218.8 %all-gather.3.cloned.1.call-start = ((), (), s32[]{:S(2)}) async-start(), calls=%async_computation.4 | async-start | bytes 6488064 | tf_op jit(solution)/shard_map/all_gather | solution.py:98
  12.0 12.4 %copy-start.4 = (bf16[64,704]{1,0:T(8,128)(2,1)S(1)}, bf16[64,704]{1,0:T(8,128)(2,1)}, u32[]{:S(2)}) copy-start(bf16[64,704]{1,0:T(8,128)(2,1)} %param.21) | copy-start | bytes 270340
  12.0 12.4 %copy-start.5 = (bf16[64,704]{1,0:T(8,128)(2,1)S(1)}, bf16[64,704]{1,0:T(8,128)(2,1)}, u32[]{:S(2)}) copy-start(bf16[64,704]{1,0:T(8,128)(2,1)} %param.22) | copy-start | bytes 270340
  12.0 12.4 %copy-start.6 = (bf16[704,64]{0,1:T(8,128)(2,1)S(1)}, bf16[704,64]{0,1:T(8,128)(2,1)}, u32[]{:S(2)}) copy-start(bf16[704,64]{0,1:T(8,128)(2,1)} %param.23) | copy-start | bytes 270340
  12.0 13.3 %copy-start.3 = (bf16[384,256]{1,0:T(8,128)(2,1)S(1)}, bf16[384,256]{1,0:T(8,128)(2,1)}, u32[]{:S(2)}) copy-start(bf16[384,256]{1,0:T(8,128)(2,1)} %param.14) | copy-start | bytes 589828
  12.0 186.0 %all-to-all-start = ((bf16[32,384,256]{1,2,0:T(8,128)(2,1)}), bf16[32,384,256]{1,2,0:T(8,128)(2,1)}, u32[]{:S(2)}, u32[]{:S(2)}) async-start(bf16[32,384,256]{1,2,0:T(8,128)(2,1)} %stack.2), calls=%async_computation | async-start | bytes 12582912 | tf_op jit(solution)/shard_map/all_to_all | solution.py:96
  24.3 393.0 %all-gather.5.cloned.1.call-start = ((), (), s32[]{:S(2)}) async-start(), calls=%async_computation.5 | async-start | bytes 9191424 | tf_op jit(solution)/shard_map/all_gather | solution.py:43
  241.3 7.0 %copy-start.1 = (f32[2,2,1536,384]{3,2,1,0:T(8,128)S(1)}, f32[2,2,1536,384]{3,2,1,0:T(8,128)}, u32[]{:S(2)}) copy-start(f32[2,2,1536,384]{3,2,1,0:T(8,128)} %get-tuple-element.149) | copy-start | bytes 28311556 | tf_op jit(solution)/shard_map/while
  257.2 7.2 %copy-start.1 = (f32[2,2,1536,384]{3,2,1,0:T(8,128)S(1)}, f32[2,2,1536,384]{3,2,1,0:T(8,128)}, u32[]{:S(2)}) copy-start(f32[2,2,1536,384]{3,2,1,0:T(8,128)} %get-tuple-element.149) | copy-start | bytes 28311556 | tf_op jit(solution)/shard_map/while
  273.3 7.4 %copy-start.1 = (f32[2,2,1536,384]{3,2,1,0:T(8,128)S(1)}, f32[2,2,1536,384]{3,2,1,0:T(8,128)}, u32[]{:S(2)}) copy-start(f32[2,2,1536,384]{3,2,1,0:T(8,128)} %get-tuple-element.149) | copy-start | bytes 28311556 | tf_op jit(solution)/shard_map/while
  289.7 7.1 %copy-start.1 = (f32[2,2,1536,384]{3,2,1,0:T(8,128)S(1)}, f32[2,2,1536,384]{3,2,1,0:T(8,128)}, u32[]{:S(2)}) copy-start(f32[2,2,1536,384]{3,2,1,0:T(8,128)} %get-tuple-element.149) | copy-start | bytes 28311556 | tf_op jit(solution)/shard_map/while
  305.7 7.0 %copy-start.1 = (f32[2,2,1536,384]{3,2,1,0:T(8,128)S(1)}, f32[2,2,1536,384]{3,2,1,0:T(8,128)}, u32[]{:S(2)}) copy-start(f32[2,2,1536,384]{3,2,1,0:T(8,128)} %get-tuple-element.149) | copy-start | bytes 28311556 | tf_op jit(solution)/shard_map/while
  321.6 7.0 %copy-start.1 = (f32[2,2,1536,384]{3,2,1,0:T(8,128)S(1)}, f32[2,2,1536,384]{3,2,1,0:T(8,128)}, u32[]{:S(2)}) copy-start(f32[2,2,1536,384]{3,2,1,0:T(8,128)} %get-tuple-element.149) | copy-start | bytes 28311556 | tf_op jit(solution)/shard_map/while
  337.5 7.0 %copy-start.1 = (f32[2,2,1536,384]{3,2,1,0:T(8,128)S(1)}, f32[2,2,1536,384]{3,2,1,0:T(8,128)}, u32[]{:S(2)}) copy-start(f32[2,2,1536,384]{3,2,1,0:T(8,128)} %get-tuple-element.149) | copy-start | bytes 28311556 | tf_op jit(solution)/shard_map/while
  353.4 7.0 %copy-start.1 = (f32[2,2,1536,384]{3,2,1,0:T(8,128)S(1)}, f32[2,2,1536,384]{3,2,1,0:T(8,128)}, u32[]{:S(2)}) copy-start(f32[2,2,1536,384]{3,2,1,0:T(8,128)} %get-tuple-element.149) | copy-start | bytes 28311556 | tf_op jit(solution)/shard_map/while
  363.1 0.7 copy-start.8
  363.1 0.8 copy-start.9
  364.7 28.2 %copy-start.2 = (bf16[48,2048]{1,0:T(8,128)(2,1)S(1)}, bf16[48,2048]{1,0:T(8,128)(2,1)}, u32[]{:S(2)}) copy-start(bf16[48,2048]{1,0:T(8,128)(2,1)} %param.13) | copy-start | bytes 589828
  364.7 28.3 %copy-start.7 = (f32[2048]{0:T(1024)S(1)}, f32[2048]{0:T(1024)}, u32[]{:S(2)}) copy-start(f32[2048]{0:T(1024)} %param.20) | copy-start | bytes 24580
Sparse Core Ops, SparseCore 0:
  9.9 180.8 all-gather.2
  193.4 108.8 all-gather.4
